TPU v7x, 1024 devices: a whole 4x8x16 slice. The times are simulated.
1024 devices in a mesh: ep: 32 (over z, core), tp: 32 (over y, x).
Axes of the slice: x: 4, y: 8, z: 16, core: 2. Of those that a mesh axis runs over, the one named last changes fastest.
Arguments:
- tokens: bfloat16 [8192, 2048], P('ep'), may hold values from -6 to 6
- gate_proj: bfloat16 [32, 2048, 4096], P('ep', None, 'tp'), may hold values from -0.125 to 0.125
- up_proj: bfloat16 [32, 2048, 4096], P('ep', None, 'tp'), may hold values from -0.125 to 0.125
- down_proj: bfloat16 [32, 4096, 2048], P('ep', 'tp'), may hold values from -0.09375 to 0.09375
- side_input_weight: bfloat16 [2048, 1024], P(None, 'tp'), may hold values from -0.125 to 0.125
- dense_out: bfloat16 [1024, 2048], P(None, 'tp'), may hold values from -0.1875 to 0.1875
- dense_gate: bfloat16 [2048], replicated, may hold values from -0.125 to 0.125
- chosen_rows: int32 [32, 1024], P(None, 'ep'), may hold values from 0 to 255, as said below
- choice_weights: float32 [32, 1024], P(None, 'ep'), may hold values from 0.25 to 1
Outputs:
- mixed: bfloat16 [8192, 2048], P('ep', 'tp')
Inputs may be any that keep to these rules, and one draw needn't show every extreme that they name: `chosen_rows`: for each expert and each block of 32 columns (one index of ep), the 32 rows are distinct rows of that index's 256 tokens; every expert reads exactly 32 tokens of every index.
All inputs are finite; a program needn't handle non-finite values.
Results may differ from a plain program's by a relative error of at most 0.015.
Values may be sent and summed in bfloat16 or wider, within the bound.
A program may use at most 64 MiB of HBM per device.

v0:
```python
import jax
import jax.numpy as jnp
from jax import lax
from jax.sharding import Mesh
from jax.sharding import PartitionSpec as P

TP = ("tp_0", "tp_1")


def whole_of(x, axes, dim):
    for axis in reversed(axes):
        x = lax.all_gather(x, axis, axis=dim, tiled=True)
    return x


def summed_rows(terms, axes):
    total = terms.astype(jnp.bfloat16)
    for axis in axes:
        total = lax.psum_scatter(total, axis, scatter_dimension=0, tiled=True)
    return total.astype(jnp.float32)


def per_device(
    tokens,
    gate_proj,
    up_proj,
    down_proj,
    side_input_weight,
    dense_out,
    dense_gate,
    chosen_rows,
    choice_weights,
):
    tok_rows = tokens.shape[0]
    width = tokens.shape[1] // lax.axis_size(TP)
    column_position = lax.axis_index(TP) * width
    own_cols = lax.dynamic_slice_in_dim(tokens, column_position, width, 1)
    expert_count, slot_rows = chosen_rows.shape
    capacity = expert_count * slot_rows
    picked = jnp.take(own_cols, chosen_rows.reshape(-1), axis=0).reshape(
        expert_count, slot_rows, width
    )
    arrived = lax.all_to_all(picked, "ep", split_axis=0, concat_axis=1, tiled=True).reshape(
        capacity, width
    )
    w_gate = gate_proj[0]
    w_up = up_proj[0]
    w_down = down_proj[0]
    piece = whole_of(arrived, TP, 1)
    gate_val = jnp.dot(piece, w_gate, preferred_element_type=jnp.float32)
    up_val = jnp.dot(piece, w_up, preferred_element_type=jnp.float32)
    hidden = (jax.nn.silu(gate_val) * up_val).astype(jnp.bfloat16)
    summed = summed_rows(
        lax.dot_general(
            w_down, hidden, (((0,), (1,)), ((), ())), preferred_element_type=jnp.float32
        ),
        TP,
    ).astype(jnp.bfloat16)
    returned = lax.all_to_all(summed, "ep", split_axis=1, concat_axis=1, tiled=True)
    hits = (
        chosen_rows.reshape(-1)[:, None] == jnp.arange(tok_rows, dtype=jnp.int32)[None, :]
    ).astype(jnp.bfloat16)
    scaled = returned.astype(jnp.float32) * choice_weights.reshape(-1)[None, :]
    high_part = scaled.astype(jnp.bfloat16)
    lower_half = (scaled - high_part.astype(jnp.float32)).astype(jnp.bfloat16)
    contract = (((0,), (1,)), ((), ()))
    routed = lax.dot_general(
        hits, high_part, contract, preferred_element_type=jnp.float32
    ) + lax.dot_general(hits, lower_half, contract, preferred_element_type=jnp.float32)
    dense_hidden = jax.nn.silu(
        jnp.dot(tokens, side_input_weight, preferred_element_type=jnp.float32)
    ).astype(jnp.bfloat16)
    dense_val = jnp.dot(
        whole_of(dense_hidden, TP, 1), dense_out, preferred_element_type=jnp.float32
    )
    side_gate = jax.nn.sigmoid(jnp.dot(tokens, dense_gate, preferred_element_type=jnp.float32))
    return (routed + side_gate[:, None] * dense_val).astype(jnp.bfloat16)


def solution(mesh):
    torus = Mesh(mesh.devices.reshape(mesh.shape["ep"], 8, 4), ("ep", "tp_0", "tp_1"))
    return jax.shard_map(
        per_device,
        mesh=torus,
        in_specs=(
            P("ep", None),
            P("ep", None, TP),
            P("ep", None, TP),
            P("ep", TP, None),
            P(None, TP),
            P(None, TP),
            P(),
            P(None, "ep"),
            P(None, "ep"),
        ),
        out_specs=P("ep", TP),
        check_vma=False,
    )
```

profile of v0, /device:TPU:16, one launch (start us, length us, event | category | flops | bytes accessed | tf_op | source)
XLA Modules:
  0.0 288.1 jit_solution(10347710762637309285)
XLA Ops:
  6.5 0.0 copy-start
  6.5 0.0 all-gather.2.cloned.1.call-start
  6.5 0.9 reshape.57
  7.5 0.7 compare_and_fusion
  8.2 0.0 copy-done
  8.2 0.1 constant_dynamic-slice_fusion
  8.3 3.2 %gather_fusion = bf16[1024,64]{1,0:T(8,128)(2,1)S(1)} fusion(bf16[256,64]{1,0:T(8,128)(2,1)S(1)} %constant_dynamic-slice_fusion, s32[1024]{0:T(1024)S(1)} %broadcast_clamp_fusion), kind=kCustom, calls=%fused_computation | custom fusion | bytes 266240 | tf_op jit(solution)/shard_map/jit(_take)/gather | solution.py:40
  11.5 0.2 broadcast_select_fusion
  11.7 0.0 copy-start.2
  11.8 0.0 copy-start.3
  11.8 0.2 reshape.72
  12.0 36.3 %all_to_all.18 = bf16[32,2,1024]{2,1,0:T(2,128)(2,1)S(1)} all-to-all(bf16[32,2,1024]{2,1,0:T(2,128)(2,1)S(1)} %reshape.72), channel_id=1, replica_groups=mesh['ep'=32,'tp_0'=8,'tp_1'=4] {'ep'}, dimensions={0} | all-to-all | bytes 262144 | tf_op jit(solution)/shard_map/all_to_all | solution.py:43
  48.2 0.2 reshape.73
  48.5 0.1 copy.11
  48.6 13.9 %all_gather.12 = bf16[1024,256]{0,1:T(8,128)(2,1)} all-gather(bf16[1024,64]{0,1:T(8,128)(2,1)S(1)} %copy.11), channel_id=1, replica_groups=mesh['ep'=32,'tp_0'=8,'tp_1'=4] {'tp_1'}, dimensions={1}, use_global_device_ids=true | all-gather | bytes 655360 | tf_op jit(solution)/shard_map/all_gather | solution.py:12
  62.5 0.0 all-gather.2.cloned.1.call-update
  62.5 0.0 reduce-scatter.5.cloned.1.call-start
  62.6 51.8 %all-gather.2.cloned.1.call-done = bf16[1024,2048]{0,1:T(8,128)(2,1)} async-done(((bf16[1024,256]{0,1:T(8,128)(2,1)}), bf16[1024,2048]{0,1:T(8,128)(2,1)}) %all-gather.2.cloned.1.call-update) | async-done | bytes 4194320 | tf_op jit(solution)/shard_map/all_gather | solution.py:12
  114.4 0.0 copy-done.1
  114.4 3.5 %fusion.10 = f32[1024,128]{1,0:T(8,128)S(1)} fusion(bf16[1024,2048]{0,1:T(8,128)(2,1)} %all-gather.2.cloned.1.call-done, bf16[1,2048,128]{2,1,0:T(8,128)(2,1)S(1)} %copy-done.1), kind=kOutput, calls=%fused_computation.16 | convolution fusion | flops 536870912 | bytes 5242880 | tf_op jit(solution)/shard_map/dot_general | solution.py:50
  117.8 0.0 copy-done.2
  117.9 0.0 copy-done.3
  117.9 8.5 %convert_bitcast_fusion = bf16[2048,1024]{0,1:T(8,128)(2,1)} fusion(bf16[1024,2048]{0,1:T(8,128)(2,1)} %all-gather.2.cloned.1.call-done, bf16[1,128,2048]{2,1,0:T(8,128)(2,1)S(1)} %copy-done.2, bf16[1,2048,128]{2,1,0:T(8,128)(2,1)S(1)} %copy-done.3, f32[1024,128]{1,0:T(8,128)S(1)} %fusion.10), kind=kOutput, calls=%fused_computation.1 | convolution fusion | flops 1076625408 | bytes 9961472 | tf_op jit(solution)/shard_map/dot_general | solution.py:54
  126.4 0.0 reduce-scatter.5.cloned.1.call-update
  126.4 0.0 copy-start.6
  126.4 0.0 reduce-scatter.7.cloned.1.call-start
  126.5 62.4 %reduce-scatter.5.cloned.1.call-done = bf16[256,1024]{0,1:T(8,128)(2,1)} async-done(((bf16[2048,1024]{0,1:T(8,128)(2,1)}), bf16[256,1024]{0,1:T(8,128)(2,1)}) %reduce-scatter.5.cloned.1.call-update) | async-done | bytes 524304 | tf_op jit(solution)/shard_map/reduce_scatter | solution.py:19
  188.9 2.1 copy.12
  190.9 0.0 reduce-scatter.7.cloned.1.call-update
  190.9 0.0 copy-done.8
  191.0 0.0 copy-done.5
  191.0 0.4 multiply_convert_fusion
  191.4 33.8 %reduce-scatter.7.cloned.1.call-done = bf16[64,1024]{1,0:T(8,128)(2,1)} async-done(((bf16[256,1024]{1,0:T(8,128)(2,1)}), bf16[64,1024]{1,0:T(8,128)(2,1)}) %reduce-scatter.7.cloned.1.call-update) | async-done | bytes 131088
  225.2 1.1 copy.13
  226.3 0.8 reshape.74
  227.1 13.3 %all-to-all-start.1 = ((bf16[32,2,1024]{2,1,0:T(2,128)(2,1)}), bf16[32,2,1024]{2,1,0:T(2,128)(2,1)S(1)}, u32[]{:S(2)}, u32[]{:S(2)}) async-start(bf16[32,2,1024]{2,1,0:T(2,128)(2,1)} %reshape.74), calls=%async_computation.2 | async-start | bytes 262144 | tf_op jit(solution)/shard_map/all_to_all | solution.py:59
  240.4 0.4 fusion.23
  240.8 0.0 copy-done.4
  240.8 0.1 eq.15
  240.9 0.1 mul.39
  241.0 11.9 %all_gather.14 = bf16[256,128]{0,1:T(8,128)(2,1)S(1)} all-gather(bf16[256,32]{0,1:T(8,128)(2,1)S(1)} %multiply_convert_fusion), channel_id=1, replica_groups=mesh['ep'=32,'tp_0'=8,'tp_1'=4] {'tp_1'}, dimensions={1}, use_global_device_ids=true | all-gather | bytes 81920 | tf_op jit(solution)/shard_map/all_gather | solution.py:12
  252.8 26.4 %all_gather.15 = bf16[256,1024]{0,1:T(8,128)(2,1)S(1)} all-gather(bf16[256,128]{0,1:T(8,128)(2,1)S(1)} %all_gather.14), channel_id=1, replica_groups=mesh['ep'=32,'tp_0'=8,'tp_1'=4] {'tp_0'}, dimensions={1}, use_global_device_ids=true | all-gather | bytes 589824 | tf_op jit(solution)/shard_map/all_gather | solution.py:12
  279.2 0.0 all-to-all-done.1
  279.2 0.2 reshape.75
  279.4 0.2 fusion.5
  279.6 0.4 fusion.3
  280.1 0.6 convolution_add_fusion
  280.7 0.8 fusion.2
  (11 shorter events, 0.0 us)
Async XLA Ops:
  6.5 1.7 copy-start
  6.5 107.8 %copy-start.1 = (bf16[1,2048,128]{2,1,0:T(8,128)(2,1)S(1)}, bf16[1,2048,128]{2,1,0:T(8,128)(2,1)}, u32[]{:S(2)}) copy-start(bf16[1,2048,128]{2,1,0:T(8,128)(2,1)} %param.10) | copy-start | bytes 1572868
  6.5 107.8 %all-gather.2.cloned.1.call-start = ((), (), s32[]{:S(2)}) async-start(), calls=%async_computation.4 | async-start | bytes 4718592 | tf_op jit(solution)/shard_map/all_gather | solution.py:12
  11.7 106.1 %copy-start.2 = (bf16[1,128,2048]{2,1,0:T(8,128)(2,1)S(1)}, bf16[1,128,2048]{2,1,0:T(8,128)(2,1)}, u32[]{:S(2)}) copy-start(bf16[1,128,2048]{2,1,0:T(8,128)(2,1)} %param.12) | copy-start | bytes 1572868
  11.8 106.1 %copy-start.3 = (bf16[1,2048,128]{2,1,0:T(8,128)(2,1)S(1)}, bf16[1,2048,128]{2,1,0:T(8,128)(2,1)}, u32[]{:S(2)}) copy-start(bf16[1,2048,128]{2,1,0:T(8,128)(2,1)} %param.11) | copy-start | bytes 1572868
  62.5 126.3 %reduce-scatter.5.cloned.1.call-start = ((), (), s32[]{:S(2)}) async-start(), calls=%async_computation.5 | async-start | bytes 4718592 | tf_op jit(solution)/shard_map/reduce_scatter | solution.py:19
  126.4 64.5 %copy-start.8 = (bf16[2048]{0:T(1024)(128)(2,1)S(1)}, bf16[2048]{0:T(1024)(128)(2,1)}, u32[]{:S(2)}) copy-start(bf16[2048]{0:T(1024)(128)(2,1)} %param.15) | copy-start | bytes 12292
  126.4 64.6 %copy-start.5 = (bf16[2048,32]{0,1:T(8,128)(2,1)S(1)}, bf16[2048,32]{0,1:T(8,128)(2,1)}, u32[]{:S(2)}) copy-start(bf16[2048,32]{0,1:T(8,128)(2,1)} %param.13) | copy-start | bytes 393220
  126.4 114.4 %copy-start.4 = (s32[32,32]{1,0:T(8,128)S(1)}, s32[32,32]{1,0:T(8,128)}, u32[]{:S(2)}) copy-start(s32[32,32]{1,0:T(8,128)} %param.16) | copy-start | bytes 12292
  126.4 114.5 %copy-start.7 = (f32[32,32]{1,0:T(8,128)S(1)}, f32[32,32]{1,0:T(8,128)}, u32[]{:S(2)}) copy-start(f32[32,32]{1,0:T(8,128)} %param.17) | copy-start | bytes 12292
  126.4 154.3 %copy-start.6 = (bf16[1024,64]{0,1:T(8,128)(2,1)S(1)}, bf16[1024,64]{0,1:T(8,128)(2,1)}, u32[]{:S(2)}) copy-start(bf16[1024,64]{0,1:T(8,128)(2,1)} %param.14) | copy-start | bytes 393220
  126.4 98.8 %reduce-scatter.7.cloned.1.call-start = ((), (), s32[]{:S(2)}) async-start(), calls=%async_computation.6 | async-start | bytes 655360
  227.1 52.0 %all-to-all-start.1 = ((bf16[32,2,1024]{2,1,0:T(2,128)(2,1)}), bf16[32,2,1024]{2,1,0:T(2,128)(2,1)S(1)}, u32[]{:S(2)}, u32[]{:S(2)}) async-start(bf16[32,2,1024]{2,1,0:T(2,128)(2,1)} %reshape.74), calls=%async_computation.2 | async-start | bytes 262144 | tf_op jit(solution)/shard_map/all_to_all | solution.py:59
Sparse Core Ops, SparseCore 0:
  62.6 51.6 all-gather.1
  126.5 62.2 reduce-scatter.4
  192.3 32.8 reduce-scatter.6
where the time goes:
time: 289 us; the launch traced here: 288 us
  waiting for transfers between devices  148 us (51%)
  blocking collectives  88.4 us (31%)
  matrix products  14.7 us (5%)
  starting transfers between devices  13.4 us (5%)
  between operations  13.3 us (5%)
  local copies, waits for them, and re-layouts  9.15 us (3%)
    reduce_scatter x1, waiting for transfers between devices, summed_rows(): total = lax.psum_scatter(total, axis, scatter_dimension=0, tiled=True)  62.4 us
    all_gather x3, blocking collectives, whole_of(): x = lax.all_gather(x, axis, axis=dim, tiled=True)  52.1 us
    all_gather x1, waiting for transfers between devices, whole_of(): x = lax.all_gather(x, axis, axis=dim, tiled=True)  51.8 us
    all_to_all x1, blocking collectives, per_device(): lax.all_to_all(picked, 'ep', split_axis=0, concat_axis=1, tiled=True)  36.3 us
    unnamed x4, waiting for transfers between devices  33.8 us
    all_to_all x1, starting transfers between devices, per_device(): lax.all_to_all(summed, 'ep', split_axis=1, concat_axis=1, tiled=True)  13.3 us
    dot_general x1, matrix products, per_device(): lax.dot_general(w_down, hidden, (((0,), (1,)), ((), ())), preferred_eleme...  8.52 us
  transfers between devices with their start and end apart: 4, of which 3 were waited for; matrix products, arithmetic and copies ran while one was open for 0% of the time, Pallas kernels for 0%

commit v1 on v0

v1 whole, which is shorter than its diff:
```python
import functools

import jax
import jax.numpy as jnp
from jax import lax
from jax.experimental import pallas as pl
from jax.experimental.pallas import tpu as pltpu
from jax.sharding import Mesh
from jax.sharding import PartitionSpec as P

MESH = pl.DeviceIdType.MESH
F32 = jnp.float32
BF16 = jnp.bfloat16
C = 128
NX = 4


def kernel(
    cfg,
    tok_hbm, gate_hbm, up_hbm, down_hbm, side_hbm, dout_hbm, dgate_ref, rows_ref, wts_ref,
    out_ref,
    tok, side, dout, w1, wd, sel, xbuf, part, m_hi, m_lo, dh,
    na, nb, nxr, fxr, fa, fb, fin, ret, exch_out, exch_in,
    loc_sem, z_ss, z_rs, w_ss, w_rs, n_ss, n_rs, f_ss, f_rs, d_ss, d_rs,
    rn_ss, rn_rs, rf_ss, rf_rs, r_ss, r_rs, e_ss, e_rs,
):
    NZ, NY, SLOT, NEAR = cfg
    LONG, SHORT = NY // 2, NY // 2 - 1
    NR = NEAR * SLOT
    ROWS = NZ * SLOT
    FR = ROWS - NR
    D = tok.shape[1]

    z, c, y, x = (lax.axis_index(a) for a in ("z", "c", "y", "x"))
    q = x // 2
    xn = NX - 1 - x
    xp = x + 1 - 2 * (x % 2)
    g = ((x + 1) // 2) % 2
    holder = c == g
    sgn = 1 - 2 * c

    def yy(j):
        return lax.rem(y + sgn * j + 2 * NY, NY)

    def zz(j):
        return lax.rem(z + j + 2 * NZ, NZ)

    def z_off(i):
        return ((i + 1) // 2) * (1 - 2 * (i % 2))

    def col(yv, qv):
        return pl.ds(pl.multiple_of(yv * 2 * C + qv * C, C), C)

    def col2(yv):
        return pl.ds(pl.multiple_of(yv * 2 * C, 2 * C), 2 * C)

    near, far = pl.ds(0, NR), pl.ds(NR, FR)
    toA, toB = {"y": yy(1)}, {"y": yy(-1)}
    toN, toP, toS = {"x": xn}, {"x": xp}, {"c": 1 - c}

    def rc(src, dst, ss, rs, dev):
        return pltpu.make_async_remote_copy(
            src_ref=src, dst_ref=dst, send_sem=ss, recv_sem=rs, device_id=dev, device_id_type=MESH
        )

    sent = []

    def send(src, dst, ss, rs, dev):
        cp = rc(src, dst, ss, rs, dev)
        cp.start()
        sent.append(cp)

    def arrive(dst, ss, rs):
        rc(dst, dst, ss, rs, toS).wait_recv()

    barrier = pltpu.get_barrier_semaphore()
    for dev in (toA, toB, toN, toP, toS):
        pl.semaphore_signal(barrier, inc=1, device_id=dev, device_id_type=MESH)

    @pl.loop(1, NZ)
    def _(k):
        pl.semaphore_signal(barrier, inc=1, device_id={"z": zz(k)}, device_id_type=MESH)

    l_tok = pltpu.make_async_copy(tok_hbm, tok, loc_sem.at[0])
    l_side = pltpu.make_async_copy(side_hbm, side, loc_sem.at[1])
    l_dout = pltpu.make_async_copy(dout_hbm, dout, loc_sem.at[2])
    l_tok.start()
    l_side.start()
    l_dout.start()
    own_w = (gate_hbm.at[0], up_hbm.at[0], down_hbm.at[0])

    def w_dst(b):
        return (w1.at[b, :, pl.ds(0, C)], w1.at[b, :, pl.ds(C, C)], wd.at[b])

    @pl.when(holder)
    def _():
        for i in range(3):
            pltpu.make_async_copy(own_w[i], w_dst(0)[i], w_rs.at[i]).start()

    ids = rows_ref[pl.ds(g, 1), :]
    hit = lax.broadcasted_iota(jnp.int32, (tok.shape[0], ROWS), 0) == ids
    l_tok.wait()
    picked = lax.dot_general(
        jnp.where(hit, 1.0, 0.0).astype(BF16), tok[:, col(y, q)], (((0,), (0,)), ((), ())),
        preferred_element_type=F32,
    )
    sel[...] = picked.astype(BF16).reshape(NZ, SLOT, C)
    wts = wts_ref[pl.ds(g, 1), :]
    w_hi = wts.astype(BF16).astype(F32)
    w_lo = wts - w_hi
    m_hi[...] = jnp.where(hit, w_hi, 0.0).astype(BF16)
    m_lo[...] = jnp.where(hit, w_lo, 0.0).astype(BF16)

    l_side.wait()
    dpre = jnp.dot(tok[...], side[...], preferred_element_type=F32)
    dpre = dpre * (1.0 / (1.0 + jnp.exp(-dpre)))
    dh[x, y] = dpre.T.astype(BF16)

    pl.semaphore_wait(barrier, 5 + NZ - 1)

    @pl.loop(1, NZ)
    def _(i):
        dest = zz(z_off(i))
        rc(
            sel.at[dest], xbuf.at[pl.ds(pl.multiple_of(i * SLOT, SLOT), SLOT), col(y, q)],
            z_ss.at[i], z_rs.at[i], {"z": dest},
        ).start()

    xbuf[pl.ds(0, SLOT), col(y, q)] = sel[z]

    @pl.when(holder)
    def _():
        for i in range(3):
            rc(own_w[i], w_dst(0)[i], w_ss.at[i], w_rs.at[i], toS).start()

    @pl.when(jnp.logical_not(holder))
    def _():
        for i in range(3):
            rc(own_w[i], w_dst(1)[i], w_ss.at[i], w_rs.at[3 + i], toP).start()

    def z_arrive(lo, hi):
        @pl.loop(lo, hi)
        def _(i):
            arrive(
                xbuf.at[pl.ds(pl.multiple_of(i * SLOT, SLOT), SLOT), col(y, q)],
                z_ss.at[i], z_rs.at[i],
            )

    z_arrive(1, NEAR)
    blk = xbuf.at[near, col(y, q)]
    send(blk, blk, n_ss.at[0], n_rs.at[0], toN)
    arrive(xbuf.at[near, col(y, 1 - q)], n_ss.at[0], n_rs.at[0])

    def n_send(yv, way, s):
        blk = xbuf.at[near, col2(yv)]
        k = 1 + way * LONG + s
        dev = toB if way else toA
        send(blk, blk, n_ss.at[k], n_rs.at[k], dev)
        send(dh.at[x, yv], dh.at[x, yv], d_ss.at[k], d_rs.at[k], dev)

    def n_arrive(yv, way, s):
        blk = xbuf.at[near, col2(yv)]
        k = 1 + way * LONG + s
        arrive(blk, n_ss.at[k], n_rs.at[k])
        arrive(dh.at[x, yv], d_ss.at[k], d_rs.at[k])

    n_send(y, 0, 0)
    n_send(y, 1, 0)

    def f_send(yv, way, s):
        blk = xbuf.at[far, col(yv, q)]
        k = way * LONG + s
        send(blk, blk, f_ss.at[k], f_rs.at[k], toB if way else toA)

    def f_arrive(yv, way, s):
        k = way * LONG + s
        arrive(xbuf.at[far, col(yv, q)], f_ss.at[k], f_rs.at[k])

    def fx_send(yv, k):
        blk = xbuf.at[far, col(yv, q)]
        send(blk, blk, f_ss.at[NY + k], f_rs.at[NY + k], toN)

    def fx_arrive(yv, k):
        arrive(xbuf.at[far, col(yv, 1 - q)], f_ss.at[NY + k], f_rs.at[NY + k])

    z_arrive(NEAR, NZ)
    f_send(y, 0, 0)
    f_send(y, 1, 0)
    fx_send(y, 0)
    for s in range(1, LONG + 1):
        ya, yb = yy(-s), yy(s)
        n_arrive(ya, 0, s - 1)
        if s < LONG:
            n_send(ya, 0, s)
        if s <= SHORT:
            n_arrive(yb, 1, s - 1)
            if s < SHORT:
                n_send(yb, 1, s)
        f_arrive(ya, 0, s - 1)
        if s < LONG:
            f_send(ya, 0, s)
        fx_send(ya, s)
        if s <= SHORT:
            f_arrive(yb, 1, s - 1)
            if s < SHORT:
                f_send(yb, 1, s)
            fx_send(yb, LONG + s)
    send(dh.at[x], dh.at[x], d_ss.at[0], d_rs.at[0], toN)

    @pl.when(holder)
    def _():
        for i in range(3):
            pltpu.make_async_copy(own_w[i], w_dst(0)[i], w_rs.at[i]).wait()
        for i in range(3):
            arrive(w_dst(1)[i], w_ss.at[i], w_rs.at[3 + i])
            rc(w_dst(1)[i], w_dst(1)[i], w_ss.at[3 + i], w_rs.at[3 + i], toS).start()

    @pl.when(jnp.logical_not(holder))
    def _():
        for i in range(3):
            arrive(w_dst(0)[i], w_ss.at[i], w_rs.at[i])
            arrive(w_dst(1)[i], w_ss.at[i], w_rs.at[3 + i])

    def experts(rows):
        halves = []
        for b in range(2):
            gu = jnp.dot(xbuf[rows, :], w1[b], preferred_element_type=F32)
            gv, uv = gu[:, :C], gu[:, C:]
            halves.append((gv * (1.0 / (1.0 + jnp.exp(-gv))) * uv).astype(BF16))
        hidden = jnp.concatenate(halves, axis=1)
        width = 512
        for n in range(D // width):
            cols = pl.ds(n * width, width)
            wdn = wd[:, :, cols].reshape(2 * C, width)
            part[rows, cols] = jnp.dot(hidden, wdn, preferred_element_type=F32).astype(BF16)

    def add(*terms):
        total = terms[0].astype(F32)
        for t in terms[1:]:
            total = total + t.astype(F32)
        return total.astype(BF16)

    experts(near)

    def rn_send(src, way, s):
        k = 1 + way * LONG + s
        dst = nb.at[s] if way else na.at[s]
        send(src, dst, rn_ss.at[k], rn_rs.at[k], toB if way else toA)

    def rn_arrive(way, s):
        k = 1 + way * LONG + s
        arrive(nb.at[s] if way else na.at[s], rn_ss.at[k], rn_rs.at[k])

    rn_send(part.at[near, col2(yy(LONG))], 0, 0)
    rn_send(part.at[near, col2(yy(-SHORT))], 1, 0)

    for k in range(NY):
        fx_arrive(yy(-k) if k <= LONG else yy(k - LONG), k)
    experts(far)

    def rx_index(j):
        return j if j >= 0 else LONG - j

    order = [LONG]
    for j in range(SHORT, 0, -1):
        order += [-j, j]
    order += [0]
    for j in order:
        k = rx_index(j)
        send(part.at[far, col(yy(j), 1 - q)], fxr.at[k], rf_ss.at[NY + k], rf_rs.at[NY + k], toN)

    def rf_send(src, way, s):
        k = way * LONG + s
        dst = fb.at[s] if way else fa.at[s]
        send(src, dst, rf_ss.at[k], rf_rs.at[k], toB if way else toA)

    def rf_arrive(way, s):
        k = way * LONG + s
        arrive(fb.at[s] if way else fa.at[s], rf_ss.at[k], rf_rs.at[k])

    def rx_arrive(j):
        k = rx_index(j)
        arrive(fxr.at[k], rf_ss.at[NY + k], rf_rs.at[NY + k])
        return fxr[k], part[far, col(yy(j), q)]

    fxr[LONG] = add(*rx_arrive(LONG))
    rf_send(fxr.at[LONG], 0, 0)
    fxr[LONG + SHORT] = add(*rx_arrive(-SHORT))
    rf_send(fxr.at[LONG + SHORT], 1, 0)

    for s in range(1, LONG):
        rn_arrive(0, s - 1)
        na[s - 1] = add(na[s - 1], part[near, col2(yy(LONG - s))])
        rn_send(na.at[s - 1], 0, s)
        if s < SHORT:
            rn_arrive(1, s - 1)
            nb[s - 1] = add(nb[s - 1], part[near, col2(yy(s - SHORT))])
            rn_send(nb.at[s - 1], 1, s)
        rf_arrive(0, s - 1)
        fa[s - 1] = add(fa[s - 1], *rx_arrive(LONG - s))
        rf_send(fa.at[s - 1], 0, s)
        if s < SHORT:
            rf_arrive(1, s - 1)
            fb[s - 1] = add(fb[s - 1], *rx_arrive(s - SHORT))
            rf_send(fb.at[s - 1], 1, s)

    rn_arrive(0, LONG - 1)
    rn_arrive(1, SHORT - 1)
    na[LONG - 1] = add(na[LONG - 1], nb[SHORT - 1], part[near, col2(y)])
    send(
        na.at[LONG - 1, :, pl.ds(pl.multiple_of((1 - q) * C, C), C)], nxr, rn_ss.at[0], rn_rs.at[0], toN
    )
    rf_arrive(0, LONG - 1)
    rf_arrive(1, SHORT - 1)
    fin[far, :] = add(fa[LONG - 1], fb[SHORT - 1], *rx_arrive(0))

    def z_return(lo, hi):
        @pl.loop(lo, hi)
        def _(i):
            rc(
                fin.at[pl.ds(pl.multiple_of(i * SLOT, SLOT), SLOT), :], ret.at[z],
                r_ss.at[i], r_rs.at[i], {"z": zz(-z_off(i))},
            ).start()

    z_return(NEAR, NZ)
    arrive(nxr, rn_ss.at[0], rn_rs.at[0])
    mine = na[LONG - 1, :, pl.ds(pl.multiple_of(q * C, C), C)]
    fin[near, :] = add(mine, nxr[...])
    z_return(1, NEAR)
    ret[z] = fin[pl.ds(0, SLOT), :]

    arrive(dh.at[xn], d_ss.at[0], d_rs.at[0])
    send(dh.at[x], dh.at[x], d_ss.at[NY], d_rs.at[NY], toP)
    send(dh.at[xn], dh.at[xn], d_ss.at[NY + 1], d_rs.at[NY + 1], toP)
    arrive(dh.at[xp], d_ss.at[NY], d_rs.at[NY])
    arrive(dh.at[NX - 1 - xp], d_ss.at[NY + 1], d_rs.at[NY + 1])
    l_dout.wait()
    dense = None
    for xv in range(NX):
        term = lax.dot_general(
            dh[xv].reshape(NY * 32, tok.shape[0]), dout[:, xv].reshape(NY * 32, 64),
            (((0,), (0,)), ((), ())), preferred_element_type=F32,
        )
        dense = term if dense is None else dense + term
    logit = jnp.sum(tok[...].astype(F32) * dgate_ref[...].astype(F32), axis=1, keepdims=True)
    dense = dense * (1.0 / (1.0 + jnp.exp(-logit)))

    @pl.loop(1, NZ)
    def _(i):
        arrive(ret.at[zz(z_off(i))], r_ss.at[i], r_rs.at[i])

    back = ret[...].reshape(ROWS, C)
    routed = jnp.dot(m_hi[...], back, preferred_element_type=F32) + jnp.dot(
        m_lo[...], back, preferred_element_type=F32
    )
    exch_out[...] = routed.astype(BF16)
    send(exch_out, exch_in, e_ss, e_rs, toP)
    arrive(exch_in, e_ss, e_rs)
    total = routed + exch_in[...].astype(F32)
    total = jnp.where(x % 2 == 1, pltpu.roll(total, C // 2, 1), total)
    out_ref[...] = (total[:, : C // 2] + dense).astype(BF16)

    for cp in sent:
        cp.wait_send()

    @pl.loop(1, NZ)
    def _(i):
        rc(sel.at[0], sel.at[0], z_ss.at[i], z_rs.at[i], toS).wait_send()
        rc(ret.at[0], ret.at[0], r_ss.at[i], r_rs.at[i], toS).wait_send()

    for i in range(3):
        rc(own_w[i], w_dst(0)[i], w_ss.at[i], w_rs.at[i], toS).wait_send()

    @pl.when(holder)
    def _():
        for i in range(3):
            rc(w_dst(1)[i], w_dst(1)[i], w_ss.at[3 + i], w_rs.at[3 + i], toS).wait_send()


def per_device(sizes, near, tokens, gate, up, down, side, dout, dgate, rows, wts):
    NZ, NY = sizes
    T, D = tokens.shape
    slot = rows.shape[1]
    n_rows = NZ * slot
    NR = near * slot
    FR = n_rows - NR
    LONG, SHORT = NY // 2, NY // 2 - 1

    def by_group(a):
        return a.reshape(NZ, 2, slot).transpose(1, 0, 2).reshape(2, n_rows)

    any_ = pl.BlockSpec(memory_space=pl.ANY)
    vmem = pl.BlockSpec(memory_space=pltpu.VMEM)
    dma = pltpu.SemaphoreType.DMA
    return pl.pallas_call(
        functools.partial(kernel, (NZ, NY, slot, near)),
        out_shape=jax.ShapeDtypeStruct((T, 64), BF16),
        in_specs=[any_] * 6 + [vmem] * 3,
        out_specs=vmem,
        scratch_shapes=[
            pltpu.VMEM((T, D), BF16),
            pltpu.VMEM((D, 32), BF16),
            pltpu.VMEM((NY, NX, 32, 64), BF16),
            pltpu.VMEM((2, D, 2 * C), BF16),
            pltpu.VMEM((2, C, D), BF16),
            pltpu.VMEM((NZ, slot, C), BF16),
            pltpu.VMEM((n_rows, D), BF16),
            pltpu.VMEM((n_rows, D), BF16),
            pltpu.VMEM((T, n_rows), BF16),
            pltpu.VMEM((T, n_rows), BF16),
            pltpu.VMEM((NX, NY, 32, T), BF16),
            pltpu.VMEM((LONG, NR, 2 * C), BF16),
            pltpu.VMEM((SHORT, NR, 2 * C), BF16),
            pltpu.VMEM((NR, C), BF16),
            pltpu.VMEM((NY, FR, C), BF16),
            pltpu.VMEM((LONG, FR, C), BF16),
            pltpu.VMEM((SHORT, FR, C), BF16),
            pltpu.VMEM((n_rows, C), BF16),
            pltpu.VMEM((NZ, slot, C), BF16),
            pltpu.VMEM((T, C), BF16),
            pltpu.VMEM((T, C), BF16),
            dma((3,)),
            dma((NZ,)), dma((NZ,)),
            dma((6,)), dma((6,)),
            dma((NY,)), dma((NY,)),
            dma((2 * NY,)), dma((2 * NY,)),
            dma((NY + 2,)), dma((NY + 2,)),
            dma((NY,)), dma((NY,)),
            dma((2 * NY,)), dma((2 * NY,)),
            dma((NZ,)), dma((NZ,)),
            dma, dma,
        ],
        compiler_params=pltpu.CompilerParams(
            collective_id=0, has_side_effects=True, vmem_limit_bytes=60 * 1024 * 1024
        ),
        name="layer",
    )(
        tokens, gate, up, down, side, dout.reshape(NY, NX, 32, 64), dgate.reshape(1, D),
        by_group(rows), by_group(wts),
    )


def solution(mesh, sizes=(16, 8), near=7):
    NZ, NY = sizes
    torus = Mesh(mesh.devices.reshape(NZ, 2, NY, NX), ("z", "c", "y", "x"))
    EP, TP = ("z", "c"), ("y", "x")
    return jax.shard_map(
        functools.partial(per_device, sizes, near),
        mesh=torus,
        in_specs=(
            P(EP, None),
            P(EP, None, TP),
            P(EP, None, TP),
            P(EP, TP, None),
            P(None, TP),
            P(None, TP),
            P(),
            P(None, EP),
            P(None, EP),
        ),
        out_specs=P(EP, TP),
        check_vma=False,
    )
```

time: 289 us -> 102 us (0.35)
  the two profiles are of different devices: /device:TPU:16 before, /device:TPU:8 now
where the time goes in v1:
time: 102 us; the launch traced here: 101 us
  Pallas kernels  93.6 us (92%)
  local copies, waits for them, and re-layouts  7.7 us (8%)
    pallas_call x1, Pallas kernels, per_device(): pl.pallas_call(functools.partial(kernel, (NZ, NY, slot, near)), out_shape...  93.6 us
    unnamed x6, local copies, waits for them, and re-layouts  2.8 us
    reshape x4, local copies, waits for them, and re-layouts, by_group(): return a.reshape(NZ, 2, slot).transpose(1, 0, 2).reshape(2, n_rows)  2.07 us

profile of v1, /device:TPU:8, one launch (start us, length us, event | category | flops | bytes accessed | tf_op | source)
XLA Modules:
  0.0 101.3 jit_solution(14571850026011343435)
XLA Ops:
  0.0 1.3 %reshape.19.dgate_ref = bf16[1,2048]{1,0:T(2,128)(2,1)} reshape(bf16[2048]{0:T(1024)(128)(2,1)} %param.15) | data formatting | bytes 8192 | tf_op jit(solution)/shard_map/reshape | solution.py:438
  1.3 0.7 copy.18
  2.0 0.0 copy-start.1
  2.0 0.7 reshape.21.rows_ref
  2.7 0.0 copy-done.1
  2.7 0.7 reshape.23.wts_ref
  3.4 0.0 copy-start
  3.4 1.8 %copy.10 = bf16[1024,64]{1,0:T(8,128)(2,1)} copy(bf16[1024,64]{0,1:T(8,128)(2,1)} %param.14) | data formatting | bytes 262144 | tf_op args[5]
  5.2 0.0 copy-done
  5.2 1.0 copy.13.side_hbm
  6.2 93.6 %layer.1 = bf16[256,64]{1,0:T(8,128)(2,1)} custom-call(bf16[256,2048]{1,0:T(8,128)(2,1)} %tok_hbm.1, bf16[1,2048,128]{2,1,0:T(8,128)(2,1)} %gate_hbm.1, bf16[1,2048,128]{2,1,0:T(8,128)(2,1)} %up_hbm.1, bf16[1,128,2048]{2,1,0:T(8,128)(2,1)} %down_hbm.1, bf16[2048,32]{1,0:T(8,128)(2,1)} %copy.13.side_hbm, bf16[8,4,32,64]{3,2,1,0:T(8,128)(2,1)} %bitcast.9, ...), custom_call_target="tpu_custom_call" | custom-call | tf_op jit(solution)/shard_map/layer/pallas_call | solution.py:395
  99.8 1.5 %copy.14 = bf16[256,64]{0,1:T(8,128)(2,1)} copy(bf16[256,64]{1,0:T(8,128)(2,1)} %layer.1) | data formatting | bytes 65536 | tf_op jit(solution)/shard_map/layer/pallas_call | solution.py:395
  (1 shorter events, 0.0 us)
Async XLA Ops:
  2.0 0.7 copy-start.1
  3.4 1.8 %copy-start = (bf16[2048,32]{0,1:T(8,128)(2,1)S(1)}, bf16[2048,32]{0,1:T(8,128)(2,1)}, u32[]{:S(2)}) copy-start(bf16[2048,32]{0,1:T(8,128)(2,1)} %param.13) | copy-start | bytes 393220

commit v2 on v0

v2 whole, which is shorter than its diff:
```python
import functools

import jax
import jax.numpy as jnp
from jax import lax
from jax.experimental import pallas as pl
from jax.experimental.pallas import tpu as pltpu
from jax.sharding import Mesh
from jax.sharding import PartitionSpec as P

MESH = pl.DeviceIdType.MESH
F32 = jnp.float32
BF16 = jnp.bfloat16
C = 128
NX = 4


def kernel(
    cfg,
    tok_hbm, gate_hbm, up_hbm, down_hbm, side_hbm, dout_hbm, dgate_ref, rows_ref, wts_ref,
    out_ref,
    tok, side, dout, w1, wd, sel, sel_whole, xbuf, part, hits, m_hi, m_lo, dh, sel_far, bundle,
    na, nb, nxr, fxr, fa, fb, fin, ret, exch_out, exch_in, side_gate,
    loc_sem, l_ss, l_rs, m_ss, z_ss, z_rs, w_ss, w_rs, n_ss, n_rs, f_ss, f_rs, d_ss, d_rs,
    rn_ss, rn_rs, rf_ss, rf_rs, r_ss, r_rs, e_ss, e_rs,
):
    NZ, NY, SLOT, DIRECT, PAIRED, NEAR = cfg
    LONG, SHORT = NY // 2, NY // 2 - 1
    ROWS = NZ * SLOT
    NR, FR = 2 * NEAR * SLOT, 2 * (NZ - NEAR) * SLOT
    T, D = tok.shape

    z, c, y, x = (lax.axis_index(a) for a in ("z", "c", "y", "x"))
    q = x // 2
    xn = NX - 1 - x
    xp = x + 1 - 2 * (x % 2)
    g = ((x + 1) // 2) % 2
    hub = c == 1
    REACH = NZ // 4
    sgn = 1 - 2 * c

    def yy(j):
        return lax.rem(y + sgn * j + 2 * NY, NY)

    def zz(j):
        return lax.rem(z + j + 2 * NZ, NZ)

    def z_off(i):
        return ((i + 1) // 2) * (1 - 2 * (i % 2))

    def col(yv, qv):
        return pl.ds(pl.multiple_of(yv * 2 * C + qv * C, C), C)

    def col2(yv):
        return pl.ds(pl.multiple_of(yv * 2 * C, 2 * C), 2 * C)

    near, far = pl.ds(0, NR), pl.ds(NR, FR)
    pair_rows = pl.ds(2 * DIRECT * SLOT, 2 * (PAIRED - DIRECT) * SLOT)
    one_rows = pl.ds(2 * PAIRED * SLOT, 2 * (NZ - PAIRED) * SLOT)
    toA, toB = {"y": yy(1)}, {"y": yy(-1)}
    toN, toP, toS = {"x": xn}, {"x": xp}, {"c": 1 - c}

    def rc(src, dst, ss, rs, dev):
        return pltpu.make_async_remote_copy(
            src_ref=src, dst_ref=dst, send_sem=ss, recv_sem=rs, device_id=dev, device_id_type=MESH
        )

    sent, mine = [], []

    def send(kept, src, dst, ss, rs, dev):
        cp = rc(src, dst, ss, rs, dev)
        cp.start()
        kept.append(cp)

    def arrive(dst, ss, rs):
        rc(dst, dst, ss, rs, toS).wait_recv()

    barrier = pltpu.get_barrier_semaphore()

    def greet(dev):
        pl.semaphore_signal(barrier, inc=1, device_id=dev, device_id_type=MESH)

    for dev in (toA, toB, toN, toP, toS):
        greet(dev)

    @pl.loop(1, REACH + 1)
    def _(k):
        greet({"z": zz(k), "c": 1})
        greet({"z": zz(-k), "c": 1})

    @pl.when(hub)
    def _():
        greet({"x": xp, "c": 0})

        @pl.loop(1, REACH + 1)
        def _(k):
            greet({"z": zz(k), "c": 0})
            greet({"z": zz(-k), "c": 0})

    l_tok = pltpu.make_async_copy(tok_hbm, tok, loc_sem.at[0])
    l_side = pltpu.make_async_copy(side_hbm, side, loc_sem.at[1])
    l_dout = pltpu.make_async_copy(dout_hbm, dout, loc_sem.at[2])
    l_tok.start()
    l_side.start()
    l_dout.start()
    own_w = (gate_hbm.at[0], up_hbm.at[0], down_hbm.at[0])

    def w_dst(b):
        return (w1.at[b, :, pl.ds(0, C)], w1.at[b, :, pl.ds(C, C)], wd.at[b])

    @pl.when(jnp.logical_and(hub, g == 1))
    def _():
        for i in range(3):
            pltpu.make_async_copy(own_w[i], w_dst(0)[i], w_rs.at[i]).start()

    ids = rows_ref[pl.ds(g, NZ, stride=2), :].T
    token = lax.broadcasted_iota(jnp.int32, (SLOT, T), 1)
    for k in range(NZ):
        hits[pl.ds(k * SLOT, SLOT), :] = jnp.where(ids[:, k : k + 1] == token, 1.0, 0.0).astype(BF16)
    l_tok.wait()
    picked = jnp.dot(hits[...], tok[:, col2(y)], preferred_element_type=F32)
    sel[...] = picked.astype(BF16).reshape(NZ, SLOT, 2 * C)
    own_chunk = pl.ds(pl.multiple_of(q * C, C), C)
    for d, way in enumerate((1, -1)):
        for j in range(REACH):
            sel_far[d, j] = sel[zz(way * (REACH + 1 + j)), :, own_chunk]

    @pl.when(hub)
    def _():
        pl.semaphore_wait(barrier, 5 + 4 * REACH)

    @pl.when(jnp.logical_not(hub))
    def _():
        pl.semaphore_wait(barrier, 6 + 2 * REACH)


    def slot_rows(i, core):
        return pl.ds(pl.multiple_of((2 * i + core) * SLOT, SLOT), SLOT)

    @pl.loop(DIRECT, PAIRED)
    def _(i):
        dest = zz(z_off(i))
        rc(
            sel.at[dest], xbuf.at[slot_rows(i, c), col2(y)], z_ss.at[i], z_rs.at[2 * i + c],
            {"z": dest, "c": 1},
        ).start()

    for d, way in enumerate((1, -1)):
        send(
            sent, sel_far.at[d], bundle.at[d, c], l_ss.at[d], l_rs.at[2 * d + c],
            {"z": zz(way * REACH), "c": 1},
        )

    def w_send(b, dev):
        for i in range(3):
            rc(own_w[i], w_dst(b)[i], w_ss.at[i], w_rs.at[3 * b + i], dev).start()

    keeps = g == c

    @pl.when(jnp.logical_not(keeps))
    def _():
        w_send(1, {"x": xp, "c": 1})

    @pl.when(jnp.logical_and(keeps, jnp.logical_not(hub)))
    def _():
        w_send(0, toS)

    l_side.wait()
    transposed = (((1,), (1,)), ((), ()))
    dpre = lax.dot_general(side[...], tok[...], transposed, preferred_element_type=F32)
    dh[y, x] = (dpre * (1.0 / (1.0 + jnp.exp(-dpre)))).astype(BF16)

    def d_send(kept, yv, way, s):
        k = 1 + way * LONG + s
        blk = dh.at[yv, x]
        send(kept, blk, blk, d_ss.at[k], d_rs.at[k], toB if way else toA)

    def d_step(s):
        for way, last in ((0, LONG), (1, SHORT)):
            if s < last:
                yv = yy(s + 1) if way else yy(-s - 1)
                k = 1 + way * LONG + s
                arrive(dh.at[yv, x], d_ss.at[k], d_rs.at[k])
                if s < last - 1:
                    d_send(mine, yv, way, s + 1)

    d_send(sent, y, 0, 0)
    d_send(sent, y, 1, 0)

    for i in range(DIRECT):
        block = hits[pl.ds(pl.multiple_of(zz(z_off(i)) * SLOT, SLOT), SLOT), :]
        sel_whole[i] = jnp.dot(block, tok[...], preferred_element_type=F32).astype(BF16)

    def whole_send():
        for i in range(1, DIRECT):
            dest = zz(z_off(i))
            rc(
                sel_whole.at[i], xbuf.at[slot_rows(i, c), :], z_ss.at[i], z_rs.at[2 * i + c],
                {"z": dest, "c": 1},
            ).start()

    def d_across():
        send(mine, dh.at[:, x], dh.at[:, x], d_ss.at[0], d_rs.at[0], toN)

    def d_pair():
        arrive(dh.at[:, xn], d_ss.at[0], d_rs.at[0])
        for k, xv in ((NY, x), (NY + 1, xn)):
            send(mine, dh.at[:, xv], dh.at[:, xv], d_ss.at[k], d_rs.at[k], toP)

    def weights_of_rows():
        wts = wts_ref[pl.ds(g, NZ, stride=2), :].T
        w_hi = wts.astype(BF16).astype(F32)
        w_lo = wts - w_hi
        for k in range(NZ):
            rows = pl.ds(k * SLOT, SLOT)
            hit = hits[rows, :].astype(F32)
            m_hi[rows, :] = (hit * w_hi[:, k : k + 1]).astype(BF16)
            m_lo[rows, :] = (hit * w_lo[:, k : k + 1]).astype(BF16)
        dgate = dgate_ref[...].astype(F32)
        dgate = jnp.concatenate([dgate[k : k + 1, :] for k in range(D // C)], axis=1).astype(BF16)
        logit = lax.dot_general(dgate, tok[...], transposed, preferred_element_type=F32)
        side_gate[...] = 1.0 / (1.0 + jnp.exp(-logit))

    @pl.when(jnp.logical_not(hub))
    def _():
        mine.clear()
        rc(
            sel_whole.at[0], xbuf.at[slot_rows(0, 0), :], z_ss.at[0], z_rs.at[0], toS
        ).start()
        d_step(0)
        d_step(1)
        whole_send()
        weights_of_rows()
        for s in range(2, LONG):
            d_step(s)
        d_across()
        d_pair()
        arrive(ret.at[z], r_ss.at[0], r_rs.at[0])
        for cp in mine:
            cp.wait_send()

    @pl.when(hub)
    def _():
        mine.clear()
        xbuf[slot_rows(0, 1), :] = sel_whole[0]
        for d, way in enumerate((1, -1)):
            for core in range(2):
                arrive(bundle.at[d, core], l_ss.at[d], l_rs.at[2 * d + core])
                for j in range(REACH):
                    k = REACH + 1 + j
                    if 2 * k == NZ and d != core:
                        continue
                    i = 2 * k - 1 if d else min(2 * k, NZ - 1)
                    send(
                        mine, bundle.at[d, core, j], xbuf.at[slot_rows(i, core), col(y, q)],
                        m_ss.at[(2 * d + core) * REACH + j], z_rs.at[2 * i + core],
                        {"z": zz(way * (j + 1)), "c": 1},
                    )

        def n_send(yv, way, s):
            blk = xbuf.at[pair_rows, col2(yv)]
            k = way * LONG + s
            send(mine, blk, blk, n_ss.at[k], n_rs.at[k], toB if way else toA)

        def n_step(s):
            for way, last in ((0, LONG), (1, SHORT)):
                if s < last:
                    yv = yy(s + 1) if way else yy(-s - 1)
                    k = way * LONG + s
                    arrive(xbuf.at[pair_rows, col2(yv)], n_ss.at[k], n_rs.at[k])
                    if s < last - 1:
                        n_send(yv, way, s + 1)

        def f_send(yv, way, s):
            blk = xbuf.at[one_rows, col(yv, q)]
            k = way * LONG + s
            send(mine, blk, blk, f_ss.at[k], f_rs.at[k], toB if way else toA)

        def fx_send(yv, k):
            blk = xbuf.at[one_rows, col(yv, q)]
            send(mine, blk, blk, f_ss.at[NY + k], f_rs.at[NY + k], toN)

        def fx_arrive(yv, k):
            arrive(xbuf.at[one_rows, col(yv, 1 - q)], f_ss.at[NY + k], f_rs.at[NY + k])

        def f_step(s):
            for way, last in ((0, LONG), (1, SHORT)):
                if s < last:
                    yv = yy(s + 1) if way else yy(-s - 1)
                    k = way * LONG + s
                    arrive(xbuf.at[one_rows, col(yv, q)], f_ss.at[k], f_rs.at[k])
                    if s < last - 1:
                        f_send(yv, way, s + 1)
                    fx_send(yv, 1 + k)

        @pl.loop(DIRECT, PAIRED)
        def _(i):
            for core in range(2):
                arrive(xbuf.at[slot_rows(i, core), col2(y)], z_ss.at[i], z_rs.at[2 * i + core])

        n_send(y, 0, 0)
        n_send(y, 1, 0)

        d_step(0)
        n_step(0)

        @pl.loop(PAIRED, NZ)
        def _(i):
            for core in range(2):
                arrive(xbuf.at[slot_rows(i, core), col(y, q)], z_ss.at[i], z_rs.at[2 * i + core])

        f_send(y, 0, 0)
        f_send(y, 1, 0)
        fx_send(y, 0)
        whole_send()
        weights_of_rows()

        def experts(rows):
            halves = []
            for b in range(2):
                gu = jnp.dot(xbuf[rows, :], w1[b], preferred_element_type=F32)
                gv, uv = gu[:, :C], gu[:, C:]
                halves.append((gv * (1.0 / (1.0 + jnp.exp(-gv))) * uv).astype(BF16))
            hidden = jnp.concatenate(halves, axis=1)
            width = 512
            for n in range(D // width):
                cols = pl.ds(n * width, width)
                wdn = wd[:, :, cols].reshape(2 * C, width)
                part[rows, cols] = jnp.dot(hidden, wdn, preferred_element_type=F32).astype(BF16)

        def add(*terms):
            total = terms[0].astype(F32)
            for t in terms[1:]:
                total = total + t.astype(F32)
            return total.astype(BF16)

        def ready():
            @pl.when(g == 1)
            def _():
                for i in range(3):
                    pltpu.make_async_copy(own_w[i], w_dst(0)[i], w_rs.at[i]).wait()

            @pl.when(g == 0)
            def _():
                for i in range(3):
                    arrive(w_dst(0)[i], w_ss.at[i], w_rs.at[i])

            for i in range(3):
                arrive(w_dst(1)[i], w_ss.at[i], w_rs.at[3 + i])
            arrive(xbuf.at[slot_rows(0, 0), :], z_ss.at[0], z_rs.at[0])
            for i in range(1, DIRECT):
                for core in range(2):
                    arrive(xbuf.at[slot_rows(i, core), :], z_ss.at[i], z_rs.at[2 * i + core])

        blocks = (pl.ds(0, 2 * DIRECT * SLOT), pl.ds(2 * DIRECT * SLOT, NR - 2 * DIRECT * SLOT))

        def rn_send(src, blk, way, s):
            k = blk * NY + 1 + way * LONG + s
            dst = (nb if way else na).at[s, blocks[blk], :]
            send(mine, src, dst, rn_ss.at[k], rn_rs.at[k], toB if way else toA)

        def rn_start(blk):
            rn_send(part.at[blocks[blk], col2(yy(LONG))], blk, 0, 0)
            rn_send(part.at[blocks[blk], col2(yy(-SHORT))], blk, 1, 0)

        def rn_step(s):
            for blk, rows in enumerate(blocks):
                for way, last, buf in ((0, LONG, na), (1, SHORT, nb)):
                    if s < last:
                        k = blk * NY + 1 + way * LONG + s
                        arrive(buf.at[s, rows, :], rn_ss.at[k], rn_rs.at[k])
                        if s < last - 1:
                            j = s + 1 - SHORT if way else LONG - 1 - s
                            buf[s, rows, :] = add(buf[s, rows, :], part[rows, col2(yy(j))])
                            rn_send(buf.at[s, rows, :], blk, way, s + 1)
                if s == LONG - 1:
                    na[s, rows, :] = add(na[s, rows, :], nb[SHORT - 1, rows, :], part[rows, col2(y)])
                    k = blk * NY
                    send(
                        mine, na.at[s, rows, pl.ds(pl.multiple_of((1 - q) * C, C), C)],
                        nxr.at[rows, :], rn_ss.at[k], rn_rs.at[k], toN,
                    )

        d_step(1)
        for s in range(1, LONG):
            f_step(s - 1)
            n_step(s)
            d_step(s + 1)
            if s == max(1, LONG - 2):
                ready()
                experts(blocks[0])
                rn_start(0)
        experts(blocks[1])
        rn_start(1)
        f_step(LONG - 1)
        rn_step(0)

        for k in range(NY):
            fx_arrive(yy(-k) if k <= LONG else yy(k - LONG), k)
        experts(far)

        def rx_index(j):
            return j if j >= 0 else LONG - j

        order = [LONG]
        for j in range(SHORT, 0, -1):
            order += [-j, j]
        order += [0]
        for j in order:
            k = rx_index(j)
            send(mine, part.at[far, col(yy(j), 1 - q)], fxr.at[k], rf_ss.at[NY + k], rf_rs.at[NY + k], toN)

        def rf_send(src, way, s):
            k = way * LONG + s
            dst = fb.at[s] if way else fa.at[s]
            send(mine, src, dst, rf_ss.at[k], rf_rs.at[k], toB if way else toA)

        def rx_arrive(j):
            k = rx_index(j)
            arrive(fxr.at[k], rf_ss.at[NY + k], rf_rs.at[NY + k])
            return fxr[k], part[far, col(yy(j), q)]

        def rf_step(s):
            for way, last, buf in ((0, LONG, fa), (1, SHORT, fb)):
                if s < last:
                    k = way * LONG + s
                    if s < last - 1:
                        j = s + 1 - SHORT if way else LONG - 1 - s
                        terms = rx_arrive(j)
                    arrive(buf.at[s], rf_ss.at[k], rf_rs.at[k])
                    if s < last - 1:
                        buf[s] = add(buf[s], *terms)
                        rf_send(buf.at[s], way, s + 1)

        d_across()
        rn_step(1)
        fxr[LONG] = add(*rx_arrive(LONG))
        rf_send(fxr.at[LONG], 0, 0)
        fxr[LONG + SHORT] = add(*rx_arrive(-SHORT))
        rf_send(fxr.at[LONG + SHORT], 1, 0)

        for s in range(2, LONG):
            rn_step(s)
            rf_step(s - 2)
        rf_step(LONG - 2)

        def z_return(lo, hi):
            @pl.loop(lo, hi)
            def _(i):
                for core in range(2):
                    rc(
                        fin.at[slot_rows(i, core), :], ret.at[z], r_ss.at[2 * i + core], r_rs.at[i],
                        {"z": zz(-z_off(i)), "c": core},
                    ).start()

        for blk, rows in enumerate(blocks):
            arrive(nxr.at[rows, :], rn_ss.at[blk * NY], rn_rs.at[blk * NY])
        own_sum = na[LONG - 1, :, pl.ds(pl.multiple_of(q * C, C), C)]
        fin[near, :] = add(own_sum, nxr[...])
        z_return(1, NEAR)
        rc(fin.at[slot_rows(0, 0), :], ret.at[z], r_ss.at[0], r_rs.at[0], toS).start()
        ret[z] = fin[pl.ds(SLOT, SLOT), :]
        terms = rx_arrive(0)
        rf_step(LONG - 1)
        fin[far, :] = add(fa[LONG - 1], fb[SHORT - 1], *terms)
        z_return(NEAR, NZ)
        d_pair()

        for cp in mine:
            cp.wait_send()

    arrive(dh.at[:, xp], d_ss.at[NY], d_rs.at[NY])
    arrive(dh.at[:, NX - 1 - xp], d_ss.at[NY + 1], d_rs.at[NY + 1])
    l_dout.wait()
    dense = jnp.dot(dout[...], dh[...].reshape(NY * NX * 32, T), preferred_element_type=F32)
    dense = dense * side_gate[...]

    @pl.loop(1, NZ)
    def _(i):
        arrive(ret.at[zz(z_off(i))], r_ss.at[i], r_rs.at[i])

    back = ret[...].reshape(ROWS, C)
    first = (((0,), (0,)), ((), ()))
    routed = lax.dot_general(back, m_hi[...], first, preferred_element_type=F32) + lax.dot_general(
        back, m_lo[...], first, preferred_element_type=F32
    )
    low, high = routed[: C // 2, :], routed[C // 2 :, :]
    odd = x % 2 == 1
    exch_out[...] = jnp.where(odd, low, high)
    send(sent, exch_out, exch_in, e_ss, e_rs, toP)
    own = jnp.where(odd, high, low) + dense
    arrive(exch_in, e_ss, e_rs)
    out_ref[...] = (own + exch_in[...]).astype(BF16)

    for cp in sent:
        cp.wait_send()

    @pl.loop(1, DIRECT)
    def _(i):
        rc(sel_whole.at[0], sel_whole.at[0], z_ss.at[i], z_rs.at[i], toS).wait_send()

    @pl.loop(DIRECT, PAIRED)
    def _(i):
        rc(sel.at[0], sel.at[0], z_ss.at[i], z_rs.at[i], toS).wait_send()

    @pl.when(jnp.logical_or(g != c, c == 0))
    def _():
        for i in range(3):
            rc(own_w[i], w_dst(0)[i], w_ss.at[i], w_rs.at[i], toS).wait_send()

    @pl.when(jnp.logical_not(hub))
    def _():
        rc(sel_whole.at[0], sel_whole.at[0], z_ss.at[0], z_rs.at[0], toS).wait_send()

    @pl.when(hub)
    def _():
        rc(ret.at[0], ret.at[0], r_ss.at[0], r_rs.at[0], toS).wait_send()

        @pl.loop(2, 2 * NZ)
        def _(i):
            rc(ret.at[0], ret.at[0], r_ss.at[i], r_rs.at[0], toS).wait_send()


def per_device(sizes, split, tokens, gate, up, down, side, dout, dgate, rows, wts):
    NZ, NY = sizes
    direct, paired, near = split
    T, D = tokens.shape
    slot = rows.shape[1]
    n_rows = NZ * slot
    NR, FR = 2 * near * slot, 2 * (NZ - near) * slot
    LONG, SHORT = NY // 2, NY // 2 - 1

    any_ = pl.BlockSpec(memory_space=pl.ANY)
    vmem = pl.BlockSpec(memory_space=pltpu.VMEM)
    dma = pltpu.SemaphoreType.DMA
    return pl.pallas_call(
        functools.partial(kernel, (NZ, NY, slot) + split),
        out_shape=jax.ShapeDtypeStruct((C // 2, T), BF16),
        in_specs=[any_] * 6 + [vmem] * 3,
        out_specs=vmem,
        scratch_shapes=[
            pltpu.VMEM((T, D), BF16),
            pltpu.VMEM((32, D), BF16),
            pltpu.VMEM((64, NY * NX * 32), BF16),
            pltpu.VMEM((2, D, 2 * C), BF16),
            pltpu.VMEM((2, C, D), BF16),
            pltpu.VMEM((NZ, slot, 2 * C), BF16),
            pltpu.VMEM((direct, slot, D), BF16),
            pltpu.VMEM((2 * n_rows, D), BF16),
            pltpu.VMEM((2 * n_rows, D), BF16),
            pltpu.VMEM((n_rows, T), BF16),
            pltpu.VMEM((n_rows, T), BF16),
            pltpu.VMEM((n_rows, T), BF16),
            pltpu.VMEM((NY, NX, 32, T), BF16),
            pltpu.VMEM((2, NZ // 4, slot, C), BF16),
            pltpu.VMEM((2, 2, NZ // 4, slot, C), BF16),
            pltpu.VMEM((LONG, NR, 2 * C), BF16),
            pltpu.VMEM((SHORT, NR, 2 * C), BF16),
            pltpu.VMEM((NR, C), BF16),
            pltpu.VMEM((NY, FR, C), BF16),
            pltpu.VMEM((LONG, FR, C), BF16),
            pltpu.VMEM((SHORT, FR, C), BF16),
            pltpu.VMEM((2 * n_rows, C), BF16),
            pltpu.VMEM((NZ, slot, C), BF16),
            pltpu.VMEM((C // 2, T), F32),
            pltpu.VMEM((C // 2, T), F32),
            pltpu.VMEM((1, T), F32),
            dma((3,)),
            dma((2,)), dma((4,)), dma((NZ,)),
            dma((NZ,)), dma((2 * NZ,)),
            dma((3,)), dma((6,)),
            dma((NY,)), dma((NY,)),
            dma((2 * NY,)), dma((2 * NY,)),
            dma((NY + 2,)), dma((NY + 2,)),
            dma((2 * NY,)), dma((2 * NY,)),
            dma((2 * NY,)), dma((2 * NY,)),
            dma((2 * NZ,)), dma((NZ,)),
            dma, dma,
        ],
        compiler_params=pltpu.CompilerParams(
            collective_id=0, has_side_effects=True, vmem_limit_bytes=60 * 1024 * 1024
        ),
        name="layer",
    )(
        tokens, gate, up, down, side.T, dout.T, dgate.reshape(D // C, C), rows, wts
    ).T


def solution(mesh, sizes=(16, 8), split=(5, 9, 9)):
    NZ, NY = sizes
    torus = Mesh(mesh.devices.reshape(NZ, 2, NY, NX), ("z", "c", "y", "x"))
    EP, TP = ("z", "c"), ("y", "x")
    return jax.shard_map(
        functools.partial(per_device, sizes, split),
        mesh=torus,
        in_specs=(
            P(EP, None),
            P(EP, None, TP),
            P(EP, None, TP),
            P(EP, TP, None),
            P(None, TP),
            P(None, TP),
            P(),
            P(None, EP),
            P(None, EP),
        ),
        out_specs=P(EP, TP),
        check_vma=False,
    )
```

time: 289 us -> 89.7 us (0.31)
  the two profiles are of different devices: /device:TPU:16 before, /device:TPU:1 now
where the time goes in v2:
time: 89.7 us; the launch traced here: 89.3 us
  Pallas kernels  87.9 us (98%)
  local copies, waits for them, and re-layouts  1.38 us (2%)
    pallas_call x1, Pallas kernels, per_device(): pl.pallas_call(functools.partial(kernel, (NZ, NY, slot) + split), out_sha...  87.9 us

profile of v2, /device:TPU:1, one launch (start us, length us, event | category | flops | bytes accessed | tf_op | source)
XLA Modules:
  0.0 89.3 jit_solution(15084639092120694516)
XLA Ops:
  0.0 87.9 %layer.1 = bf16[64,256]{1,0:T(8,128)(2,1)} custom-call(bf16[256,2048]{1,0:T(8,128)(2,1)} %tok_hbm.1, bf16[1,2048,128]{2,1,0:T(8,128)(2,1)} %gate_hbm.1, bf16[1,2048,128]{2,1,0:T(8,128)(2,1)} %up_hbm.1, bf16[1,128,2048]{2,1,0:T(8,128)(2,1)} %down_hbm.1, bf16[32,2048]{1,0:T(8,128)(2,1)} %bitcast.5, bf16[64,1024]{1,0:T(8,128)(2,1)} %bitcast.6, ...), custom_call_target="tpu_custom_call" | custom-call | tf_op jit(solution)/shard_map/layer/pallas_call | solution.py:536
  87.9 1.4 %copy.11 = bf16[256,64]{0,1:T(8,128)(2,1)} copy(bf16[256,64]{0,1:T(8,128)(2,1)} %bitcast.4) | data formatting | bytes 65536

commit v3 on v2

--- a/solution.py
+++ b/solution.py
@@ -19,9 +19,9 @@
     cfg,
     tok_hbm, gate_hbm, up_hbm, down_hbm, side_hbm, dout_hbm, dgate_ref, rows_ref, wts_ref,
     out_ref,
-    tok, side, dout, w1, wd, sel, sel_whole, xbuf, part, hits, m_hi, m_lo, dh, sel_far, bundle,
+    tok, side, dout, w1, wd, sel, sel_whole, xbuf, part, hits, m_hi, m_lo, dh, dh_own, dense_val, dense_in, sel_far, bundle,
     na, nb, nxr, fxr, fa, fb, fin, ret, exch_out, exch_in, side_gate,
-    loc_sem, l_ss, l_rs, m_ss, z_ss, z_rs, w_ss, w_rs, n_ss, n_rs, f_ss, f_rs, d_ss, d_rs,
+    loc_sem, go, h_ss, h_rs, l_ss, l_rs, m_ss, z_ss, z_rs, w_ss, w_rs, n_ss, n_rs, f_ss, f_rs, d_ss, d_rs,
     rn_ss, rn_rs, rf_ss, rf_rs, r_ss, r_rs, e_ss, e_rs,
 ):
     NZ, NY, SLOT, DIRECT, PAIRED, NEAR = cfg
@@ -137,6 +137,12 @@
     def slot_rows(i, core):
         return pl.ds(pl.multiple_of((2 * i + core) * SLOT, SLOT), SLOT)
 
+    for d, way in enumerate((1, -1)):
+        send(
+            sent, sel_far.at[d], bundle.at[d, c], l_ss.at[d], l_rs.at[2 * d + c],
+            {"z": zz(way * REACH), "c": 1},
+        )
+
     @pl.loop(DIRECT, PAIRED)
     def _(i):
         dest = zz(z_off(i))
@@ -145,12 +151,6 @@
             {"z": dest, "c": 1},
         ).start()
 
-    for d, way in enumerate((1, -1)):
-        send(
-            sent, sel_far.at[d], bundle.at[d, c], l_ss.at[d], l_rs.at[2 * d + c],
-            {"z": zz(way * REACH), "c": 1},
-        )
-
     def w_send(b, dev):
         for i in range(3):
             rc(own_w[i], w_dst(b)[i], w_ss.at[i], w_rs.at[3 * b + i], dev).start()
@@ -168,24 +168,30 @@
     l_side.wait()
     transposed = (((1,), (1,)), ((), ()))
     dpre = lax.dot_general(side[...], tok[...], transposed, preferred_element_type=F32)
-    dh[y, x] = (dpre * (1.0 / (1.0 + jnp.exp(-dpre)))).astype(BF16)
-
-    def d_send(kept, yv, way, s):
-        k = 1 + way * LONG + s
-        blk = dh.at[yv, x]
-        send(kept, blk, blk, d_ss.at[k], d_rs.at[k], toB if way else toA)
+    dense_hidden = (dpre * (1.0 / (1.0 + jnp.exp(-dpre)))).astype(BF16)
+
+    @pl.when(hub)
+    def _():
+        dh_own[...] = dense_hidden
+        rc(dh_own, dh.at[1, y, x], h_ss.at[0], h_rs.at[0], toS).start()
+
+    @pl.when(jnp.logical_not(hub))
+    def _():
+        dh[0, y, x] = dense_hidden
+
+    def d_send(yv, way, s):
+        k = 2 + way * LONG + s
+        blk = dh.at[:, yv, x]
+        send(mine, blk, blk, d_ss.at[k], d_rs.at[k], toB if way else toA)
 
     def d_step(s):
         for way, last in ((0, LONG), (1, SHORT)):
             if s < last:
                 yv = yy(s + 1) if way else yy(-s - 1)
-                k = 1 + way * LONG + s
-                arrive(dh.at[yv, x], d_ss.at[k], d_rs.at[k])
+                k = 2 + way * LONG + s
+                arrive(dh.at[:, yv, x], d_ss.at[k], d_rs.at[k])
                 if s < last - 1:
-                    d_send(mine, yv, way, s + 1)
-
-    d_send(sent, y, 0, 0)
-    d_send(sent, y, 1, 0)
+                    d_send(yv, way, s + 1)
 
     for i in range(DIRECT):
         block = hits[pl.ds(pl.multiple_of(zz(z_off(i)) * SLOT, SLOT), SLOT), :]
@@ -199,13 +205,8 @@
                 {"z": dest, "c": 1},
             ).start()
 
-    def d_across():
-        send(mine, dh.at[:, x], dh.at[:, x], d_ss.at[0], d_rs.at[0], toN)
-
-    def d_pair():
-        arrive(dh.at[:, xn], d_ss.at[0], d_rs.at[0])
-        for k, xv in ((NY, x), (NY + 1, xn)):
-            send(mine, dh.at[:, xv], dh.at[:, xv], d_ss.at[k], d_rs.at[k], toP)
+    def d_column(xv, k, dev):
+        send(mine, dh.at[:, :, xv], dh.at[:, :, xv], d_ss.at[k], d_rs.at[k], dev)
 
     def weights_of_rows():
         wts = wts_ref[pl.ds(g, NZ, stride=2), :].T
@@ -227,14 +228,30 @@
         rc(
             sel_whole.at[0], xbuf.at[slot_rows(0, 0), :], z_ss.at[0], z_rs.at[0], toS
         ).start()
+        arrive(dh.at[1, y, x], h_ss.at[0], h_rs.at[0])
+        d_send(y, 0, 0)
+        d_send(y, 1, 0)
         d_step(0)
-        d_step(1)
-        whole_send()
         weights_of_rows()
-        for s in range(2, LONG):
+        for s in range(1, LONG):
+            if s == LONG - 1:
+                whole_send()
             d_step(s)
-        d_across()
-        d_pair()
+        d_column(x, 0, toP)
+        pl.semaphore_wait(go, 1)
+        d_column(x, 1, toN)
+        arrive(dh.at[:, :, xn], d_ss.at[1], d_rs.at[1])
+        d_column(xn, NY + 1, toP)
+        l_dout.wait()
+        arrive(dh.at[:, :, xp], d_ss.at[0], d_rs.at[0])
+        arrive(dh.at[:, :, NX - 1 - xp], d_ss.at[NY + 1], d_rs.at[NY + 1])
+        for core in (1, 0):
+            dense_val[core] = jnp.dot(
+                dout[...], dh[core].reshape(NY * NX * 32, T), preferred_element_type=F32
+            )
+            if core == 1:
+                send(mine, dense_val.at[1], dense_in, h_ss.at[1], h_rs.at[1], toS)
+        dense_in[...] = dense_val[0]
         arrive(ret.at[z], r_ss.at[0], r_rs.at[0])
         for cp in mine:
             cp.wait_send()
@@ -301,9 +318,6 @@
         n_send(y, 0, 0)
         n_send(y, 1, 0)
 
-        d_step(0)
-        n_step(0)
-
         @pl.loop(PAIRED, NZ)
         def _(i):
             for core in range(2):
@@ -313,6 +327,7 @@
         f_send(y, 1, 0)
         fx_send(y, 0)
         whole_send()
+        n_step(0)
         weights_of_rows()
 
         def experts(rows):
@@ -363,8 +378,8 @@
             rn_send(part.at[blocks[blk], col2(yy(LONG))], blk, 0, 0)
             rn_send(part.at[blocks[blk], col2(yy(-SHORT))], blk, 1, 0)
 
-        def rn_step(s):
-            for blk, rows in enumerate(blocks):
+        def rn_step(blk, s):
+            for rows in blocks[blk : blk + 1]:
                 for way, last, buf in ((0, LONG, na), (1, SHORT, nb)):
                     if s < last:
                         k = blk * NY + 1 + way * LONG + s
@@ -381,19 +396,17 @@
                         nxr.at[rows, :], rn_ss.at[k], rn_rs.at[k], toN,
                     )
 
-        d_step(1)
-        for s in range(1, LONG):
-            f_step(s - 1)
-            n_step(s)
-            d_step(s + 1)
-            if s == max(1, LONG - 2):
+        for s in range(LONG):
+            f_step(s)
+            if s == 1 and LONG > 2:
+                n_step(1)
+            if s == LONG - 2:
                 ready()
                 experts(blocks[0])
                 rn_start(0)
-        experts(blocks[1])
-        rn_start(1)
-        f_step(LONG - 1)
-        rn_step(0)
+                for k in range(2, LONG - 1):
+                    n_step(k)
+        rn_step(0, 0)
 
         for k in range(NY):
             fx_arrive(yy(-k) if k <= LONG else yy(k - LONG), k)
@@ -432,48 +445,55 @@
                         buf[s] = add(buf[s], *terms)
                         rf_send(buf.at[s], way, s + 1)
 
-        d_across()
-        rn_step(1)
+        n_step(LONG - 1)
+        experts(blocks[1])
+        rn_start(1)
+        rn_step(0, 1)
         fxr[LONG] = add(*rx_arrive(LONG))
         rf_send(fxr.at[LONG], 0, 0)
         fxr[LONG + SHORT] = add(*rx_arrive(-SHORT))
         rf_send(fxr.at[LONG + SHORT], 1, 0)
-
-        for s in range(2, LONG):
-            rn_step(s)
-            rf_step(s - 2)
-        rf_step(LONG - 2)
+        rn_step(1, 0)
+        if LONG > 2:
+            rn_step(0, 2)
+        for s in range(LONG - 1):
+            rf_step(s)
+            if s == 0:
+                pl.semaphore_signal(go, inc=1, device_id=toS, device_id_type=MESH)
+            if s == 1 and LONG > 3:
+                rn_step(0, 3)
+            if s + 1 < LONG - 1:
+                rn_step(1, s + 1)
 
         def z_return(lo, hi):
-            @pl.loop(lo, hi)
-            def _(i):
+            @pl.loop(0, hi - lo)
+            def _(back):
+                i = hi - 1 - back
                 for core in range(2):
                     rc(
                         fin.at[slot_rows(i, core), :], ret.at[z], r_ss.at[2 * i + core], r_rs.at[i],
                         {"z": zz(-z_off(i)), "c": core},
                     ).start()
 
-        for blk, rows in enumerate(blocks):
-            arrive(nxr.at[rows, :], rn_ss.at[blk * NY], rn_rs.at[blk * NY])
-        own_sum = na[LONG - 1, :, pl.ds(pl.multiple_of(q * C, C), C)]
-        fin[near, :] = add(own_sum, nxr[...])
-        z_return(1, NEAR)
-        rc(fin.at[slot_rows(0, 0), :], ret.at[z], r_ss.at[0], r_rs.at[0], toS).start()
-        ret[z] = fin[pl.ds(SLOT, SLOT), :]
         terms = rx_arrive(0)
         rf_step(LONG - 1)
         fin[far, :] = add(fa[LONG - 1], fb[SHORT - 1], *terms)
         z_return(NEAR, NZ)
-        d_pair()
-
+        for blk, (lo, hi) in enumerate(((0, DIRECT), (DIRECT, NEAR))):
+            rows = blocks[blk]
+            if blk == 1:
+                rn_step(1, LONG - 1)
+            arrive(nxr.at[rows, :], rn_ss.at[blk * NY], rn_rs.at[blk * NY])
+            own_sum = na[LONG - 1, rows, pl.ds(pl.multiple_of(q * C, C), C)]
+            fin[rows, :] = add(own_sum, nxr[rows, :])
+            z_return(max(lo, 1), hi)
+        rc(fin.at[slot_rows(0, 0), :], ret.at[z], r_ss.at[0], r_rs.at[0], toS).start()
+        ret[z] = fin[pl.ds(SLOT, SLOT), :]
+        l_dout.wait()
+        arrive(dense_in, h_ss.at[1], h_rs.at[1])
+        rc(dh_own, dh_own, h_ss.at[0], h_rs.at[0], toS).wait_send()
         for cp in mine:
             cp.wait_send()
-
-    arrive(dh.at[:, xp], d_ss.at[NY], d_rs.at[NY])
-    arrive(dh.at[:, NX - 1 - xp], d_ss.at[NY + 1], d_rs.at[NY + 1])
-    l_dout.wait()
-    dense = jnp.dot(dout[...], dh[...].reshape(NY * NX * 32, T), preferred_element_type=F32)
-    dense = dense * side_gate[...]
 
     @pl.loop(1, NZ)
     def _(i):
@@ -486,11 +506,11 @@
     )
     low, high = routed[: C // 2, :], routed[C // 2 :, :]
     odd = x % 2 == 1
-    exch_out[...] = jnp.where(odd, low, high)
+    exch_out[...] = jnp.where(odd, low, high).astype(BF16)
     send(sent, exch_out, exch_in, e_ss, e_rs, toP)
-    own = jnp.where(odd, high, low) + dense
+    own = jnp.where(odd, high, low) + dense_in[...] * side_gate[...]
     arrive(exch_in, e_ss, e_rs)
-    out_ref[...] = (own + exch_in[...]).astype(BF16)
+    out_ref[...] = (own + exch_in[...].astype(F32)).astype(BF16)
 
     for cp in sent:
         cp.wait_send()
@@ -551,7 +571,10 @@
             pltpu.VMEM((n_rows, T), BF16),
             pltpu.VMEM((n_rows, T), BF16),
             pltpu.VMEM((n_rows, T), BF16),
-            pltpu.VMEM((NY, NX, 32, T), BF16),
+            pltpu.VMEM((2, NY, NX, 32, T), BF16),
+            pltpu.VMEM((32, T), BF16),
+            pltpu.VMEM((2, C // 2, T), F32),
+            pltpu.VMEM((C // 2, T), F32),
             pltpu.VMEM((2, NZ // 4, slot, C), BF16),
             pltpu.VMEM((2, 2, NZ // 4, slot, C), BF16),
             pltpu.VMEM((LONG, NR, 2 * C), BF16),
@@ -562,10 +585,11 @@
             pltpu.VMEM((SHORT, FR, C), BF16),
             pltpu.VMEM((2 * n_rows, C), BF16),
             pltpu.VMEM((NZ, slot, C), BF16),
-            pltpu.VMEM((C // 2, T), F32),
-            pltpu.VMEM((C // 2, T), F32),
+            pltpu.VMEM((C // 2, T), BF16),
+            pltpu.VMEM((C // 2, T), BF16),
             pltpu.VMEM((1, T), F32),
             dma((3,)),
+            pltpu.SemaphoreType.REGULAR, dma((2,)), dma((2,)),
             dma((2,)), dma((4,)), dma((NZ,)),
             dma((NZ,)), dma((2 * NZ,)),
             dma((3,)), dma((6,)),

time: 89.7 us -> 86.5 us (0.964)
  Pallas kernels: 87.9 us -> 84.9 us
    pallas_call x1, Pallas kernels: 87.9 us -> 84.9 us  [per_device(): pl.pallas_call(functools.partial(kernel, (NZ, NY, slot) + split), out_sha...]
where the time goes in v3:
time: 86.5 us; the launch traced here: 86.3 us
  Pallas kernels  84.9 us (98%)
  local copies, waits for them, and re-layouts  1.38 us (2%)
    pallas_call x1, Pallas kernels, per_device(): pl.pallas_call(functools.partial(kernel, (NZ, NY, slot) + split), out_sha...  84.9 us

profile of v3, /device:TPU:1, one launch (start us, length us, event | category | flops | bytes accessed | tf_op | source)
XLA Modules:
  0.0 86.3 jit_solution(11644717204506285086)
XLA Ops:
  0.0 84.9 %layer.1 = bf16[64,256]{1,0:T(8,128)(2,1)} custom-call(bf16[256,2048]{1,0:T(8,128)(2,1)} %tok_hbm.1, bf16[1,2048,128]{2,1,0:T(8,128)(2,1)} %gate_hbm.1, bf16[1,2048,128]{2,1,0:T(8,128)(2,1)} %up_hbm.1, bf16[1,128,2048]{2,1,0:T(8,128)(2,1)} %down_hbm.1, bf16[32,2048]{1,0:T(8,128)(2,1)} %bitcast.5, bf16[64,1024]{1,0:T(8,128)(2,1)} %bitcast.6, ...), custom_call_target="tpu_custom_call" | custom-call | tf_op jit(solution)/shard_map/layer/pallas_call | solution.py:556
  84.9 1.4 %copy.11 = bf16[256,64]{0,1:T(8,128)(2,1)} copy(bf16[256,64]{0,1:T(8,128)(2,1)} %bitcast.4) | data formatting | bytes 65536
